TPU v7x, 32 devices: a whole 2x2x4 slice. The times are simulated.
32 devices in a mesh: sp: 8 (over z, y), tp: 4 (over x, core).
Axes of the slice: x: 2, y: 2, z: 4, core: 2. Of those that a mesh axis runs over, the one named last changes fastest.
Arguments:
- inputs: bfloat16 [8192, 4, 2048], P('sp'), may hold values from -6 to 6
- norm_gain: float32 [2048], replicated, may hold values from 0.1 to 1.9
- pool_proj: bfloat16 [2048, 1024], P(None, 'tp'), may hold values from -0.125 to 0.125
- pool_gate_proj: bfloat16 [2048, 1024], P(None, 'tp'), may hold values from -0.125 to 0.125
- pool_mix: bfloat16 [8, 128, 128], P('tp'), may hold values from -0.5 to 0.5
- query_proj: bfloat16 [2048, 1024], P(None, 'tp'), may hold values from -0.125 to 0.125
- key_proj: bfloat16 [2048, 512], P(None, 'tp'), may hold values from -0.125 to 0.125
- value_proj: bfloat16 [2048, 512], P(None, 'tp'), may hold values from -0.125 to 0.125
- attn_gate_proj: bfloat16 [2048, 1024], P(None, 'tp'), may hold values from -0.125 to 0.125
- query_gain: float32 [64], replicated, may hold values from 0.1 to 1.9
- key_gain: float32 [64], replicated, may hold values from 0.1 to 1.9
- sink_logit: float32 [16], P('tp'), may hold values from -12 to 240
- out_pool: bfloat16 [1024, 2048], P('sp'), may hold values from -0.125 to 0.125
- out_attn: bfloat16 [1024, 2048], P('sp'), may hold values from -0.125 to 0.125
Outputs:
- mixed_out: bfloat16 [8192, 4, 2048], P(('sp', 'tp'))
- log_weight_sum: float32 [8192, 4, 16], P('sp', None, 'tp')
All inputs are finite; a program needn't handle non-finite values.
Results may differ from a plain program's by a relative error of at most 0.015.
Values may be sent and summed in bfloat16 or wider, within the bound.
A program may use at most 192 MiB of HBM per device.

v0:
```python
import functools
import math

import jax
import jax.numpy as jnp
from jax import lax
from jax.experimental import pallas as pl
from jax.experimental.pallas import tpu as pltpu
from jax.sharding import PartitionSpec as P

HEADS = 16
HEAD_DIM = 64
WINDOW = 128
EPS = 1e-06
NEG = -1e30
LOG2E = math.log2(math.e)
REACH = 16
BLK = 128
F32 = jnp.float32
BF16 = jnp.bfloat16


def halo(shard, width):
    count, length = lax.axis_size("sp"), shard.shape[1]
    up = [(i, i + 1) for i in range(count - 1)]
    down = [(j, i) for i, j in up]
    before = lax.ppermute(shard[:, length - width :], "sp", up)
    after = lax.ppermute(shard[:, :width], "sp", down)
    return before, after


def head_ones(cols):
    a = lax.broadcasted_iota(jnp.int32, (cols, cols), 0) // HEAD_DIM
    b = lax.broadcasted_iota(jnp.int32, (cols, cols), 1) // HEAD_DIM
    return jnp.where(a == b, 1.0 / HEAD_DIM, 0.0).astype(BF16)


def head_norm(values, gain):
    flt = values.astype(F32)
    mean = jnp.dot((flt * flt).astype(BF16), head_ones(flt.shape[-1]), preferred_element_type=F32)
    return (flt * lax.rsqrt(mean + EPS) * gain).astype(BF16)


def silu(gate):
    flt = gate.astype(F32)
    return flt / (1.0 + jnp.exp(-flt))


def mix_kernel(
    pc, qc, kc, total_len,
    ints, floats, proj, kv_before, kv_after, pool_before, pool_after, mix, q_gain, k_gain,
    y_pool, y_attn, lse,
    keys, vals, pool_pad, bias, band,
):
    length = proj.shape[1]
    rows = y_pool.shape[2]
    n_kv = kc // HEAD_DIM
    n_q = qc // HEAD_DIM
    groups = mix.shape[0]
    chan = mix.shape[1]
    offset = ints[0]
    c_gate, c_q, c_ag, c_kv = pc, 2 * pc, 2 * pc + qc, 2 * pc + 2 * qc
    half_pad = 64

    @pl.when(pl.program_id(0) == 0)
    def _():
        i = lax.broadcasted_iota(jnp.int32, (BLK, 3 * WINDOW), 0)
        j = lax.broadcasted_iota(jnp.int32, (BLK, 3 * WINDOW), 1) - WINDOW
        dist = jnp.abs(i - j)
        for h in range(n_q):
            value = -floats[0, h] * dist.astype(F32) - floats[1, h]
            bias[h] = jnp.where(dist <= WINDOW, value, NEG)
        ti = lax.broadcasted_iota(jnp.int32, (BLK, 2 * BLK), 0)
        tj = lax.broadcasted_iota(jnp.int32, (BLK, 2 * BLK), 1) - half_pad
        rel = tj - ti
        for g in range(groups):
            hw = ints[1 + g]
            inside = (rel >= -hw) & (rel <= hw - 1)
            band[g] = jnp.where(inside, 1.0, 0.0).astype(BF16)
        edge = jnp.zeros((half_pad - REACH, pc), BF16)
        pool_pad[0 : half_pad - REACH] = edge
        pool_pad[half_pad + length + REACH :] = edge

    pool_pad[half_pad - REACH : half_pad] = pool_before[0]
    pool_pad[half_pad : half_pad + length] = proj[0, :, :pc]
    pool_pad[half_pad + length : half_pad + length + REACH] = pool_after[0]

    def fill(first, count, kv):
        normed = head_norm(kv[:, :kc], k_gain[...])
        pos = lax.broadcasted_iota(jnp.int32, (count, HEAD_DIM), 0) + (offset + first - WINDOW)
        ones = jnp.where((pos >= 0) & (pos < total_len), 1.0, 0.0).astype(BF16)
        for p in range(n_kv):
            k = normed[:, p * HEAD_DIM : (p + 1) * HEAD_DIM]
            v = kv[:, kc + p * HEAD_DIM : kc + (p + 1) * HEAD_DIM]
            keys[p, first : first + count] = jnp.concatenate([k, k], axis=1)
            vals[2 * p, first : first + count] = jnp.concatenate([v, ones], axis=1)
            vals[2 * p + 1, first : first + count] = jnp.concatenate([ones, v], axis=1)

    fill(0, WINDOW, kv_before[0])
    fill(WINDOW, length, proj[0, :, c_kv:])
    fill(WINDOW + length, WINDOW, kv_after[0])

    low = lax.broadcasted_iota(jnp.int32, (BLK, 2 * HEAD_DIM), 1) < HEAD_DIM

    def step(b, carry):
        start = pl.multiple_of(b * BLK, BLK)
        dest = start // rows
        row = pl.multiple_of(start % rows, BLK)
        here = pl.ds(start, BLK)
        gpos = offset + start + lax.broadcasted_iota(jnp.int32, (BLK, chan), 0)
        for g in range(groups):
            hw = ints[1 + g]
            cols = slice(g * chan, (g + 1) * chan)
            window = jnp.dot(band[g], pool_pad[pl.ds(start, 2 * BLK), cols], preferred_element_type=F32)
            lo = jnp.maximum(gpos - hw, 0)
            hi = jnp.minimum(gpos + hw - 1, total_len - 1)
            live = (hi - lo + 1).astype(F32)
            pooled = (window / live - proj[0, here, cols].astype(F32)).astype(BF16)
            mixed = jnp.dot(pooled, mix[g], preferred_element_type=F32)
            gate = proj[0, here, c_gate + g * chan : c_gate + (g + 1) * chan]
            y_pool[dest, 0, pl.ds(row, BLK), cols] = (mixed * silu(gate)).astype(BF16)
        queries = head_norm(proj[0, here, c_q : c_q + qc], q_gain[...])
        for p in range(n_kv):
            pair = queries[:, p * 128 : (p + 1) * 128]
            zero = jnp.zeros_like(pair)
            stacked = jnp.concatenate([jnp.where(low, pair, zero), jnp.where(low, zero, pair)], axis=0)
            span = pl.ds(start, 3 * WINDOW)
            scores = lax.dot_general(
                stacked, keys[p, span], (((1,), (1,)), ((), ())), preferred_element_type=F32
            )
            w0 = jnp.exp2(scores[:BLK] + bias[2 * p]).astype(BF16)
            w1 = jnp.exp2(scores[BLK:] + bias[2 * p + 1]).astype(BF16)
            o0 = jnp.dot(w0, vals[2 * p, span], preferred_element_type=F32)
            o1 = jnp.dot(w1, vals[2 * p + 1, span], preferred_element_type=F32)
            num = jnp.where(low, o0, o1)
            tot = jnp.where(low, o1, o0) + 1.0
            den = pltpu.roll(tot, HEAD_DIM, 1)
            gate = proj[0, here, c_ag + p * 128 : c_ag + (p + 1) * 128]
            y_attn[dest, 0, pl.ds(row, BLK), p * 128 : (p + 1) * 128] = (num / den * silu(gate)).astype(BF16)
            tt = jnp.transpose(tot)
            lse[0, 2 * p : 2 * p + 1, here] = floats[2, 2 * p] + jnp.log(tt[HEAD_DIM : HEAD_DIM + 1])
            lse[0, 2 * p + 1 : 2 * p + 2, here] = floats[2, 2 * p + 1] + jnp.log(tt[0:1])
        return carry

    lax.fori_loop(0, length // BLK, step, 0)


def out_kernel(tp, pool_rows, attn_rows, w_pool, w_attn, out):
    width = pool_rows.shape[-1]
    acc = None
    for rows_ref, w_ref in ((pool_rows, w_pool), (attn_rows, w_attn)):
        lhs = jnp.concatenate([rows_ref[p, 0] for p in range(tp)], axis=1)
        part = jnp.dot(lhs, w_ref[...], preferred_element_type=F32)
        acc = part if acc is None else acc + part
    out[0] = acc.astype(BF16)


def body(
    inputs, norm_gain, pool_proj, pool_gate_proj, pool_mix, query_proj, key_proj, value_proj,
    attn_gate_proj, query_gain, key_gain, sink_logit, out_pool, out_attn,
):
    length, seqs, model = inputs.shape
    tp = lax.axis_size("tp")
    tp_index = lax.axis_index("tp")
    offset = lax.axis_index("sp") * length
    total_len = length * lax.axis_size("sp")
    pc, qc, kc = pool_proj.shape[1], query_proj.shape[1], key_proj.shape[1]
    width = 2 * pc + 2 * qc + 2 * kc
    n_q = qc // HEAD_DIM
    n_kv = kc // HEAD_DIM
    groups = pool_mix.shape[0]
    rows = length // tp

    w_pool = lax.all_gather(out_pool, "sp", axis=0, tiled=True)
    w_attn = lax.all_gather(out_attn, "sp", axis=0, tiled=True)

    flt = inputs.astype(F32)
    scale = lax.rsqrt(jnp.mean(flt * flt, axis=-1) + EPS)
    weights = jnp.concatenate(
        [pool_proj, pool_gate_proj, query_proj, attn_gate_proj, key_proj, value_proj], axis=1
    )
    weights = (weights.astype(F32) * norm_gain[:, None]).astype(BF16)
    proj = jnp.einsum("tsd,dc->stc", inputs, weights, preferred_element_type=F32)
    proj = (proj * scale.T[:, :, None]).astype(BF16)

    kv_before, kv_after = halo(proj[:, :, 2 * pc + 2 * qc :], WINDOW)
    pool_before, pool_after = halo(proj[:, :, :pc], REACH)

    head_ids = tp_index * n_q + jnp.arange(n_q, dtype=jnp.int32)
    slopes = 2.0 ** (-8.0 * (head_ids + 1).astype(F32) / HEADS)
    floats = jnp.stack([slopes * LOG2E, sink_logit * LOG2E, sink_logit])
    half_widths = jnp.left_shift(
        jnp.int32(1), (tp_index * groups + jnp.arange(groups, dtype=jnp.int32)) % 4
    )
    ints = jnp.concatenate([offset[None].astype(jnp.int32), half_widths])
    q_gain = jnp.tile(query_gain * (HEAD_DIM**-0.5 * LOG2E), n_q)[None]
    k_gain = jnp.tile(key_gain, n_kv)[None]

    smem = pl.BlockSpec(memory_space=pltpu.SMEM)
    full = lambda shape: pl.BlockSpec(shape, lambda s: (0,) * len(shape))
    per_seq = lambda *shape: pl.BlockSpec((1,) + shape, lambda s: (s,) + (0,) * len(shape))
    y_pool, y_attn, lse = pl.pallas_call(
        functools.partial(mix_kernel, pc, qc, kc, total_len),
        grid=(seqs,),
        in_specs=[
            smem, smem,
            per_seq(length, width),
            per_seq(WINDOW, 2 * kc), per_seq(WINDOW, 2 * kc),
            per_seq(REACH, pc), per_seq(REACH, pc),
            full(pool_mix.shape), full((1, qc)), full((1, kc)),
        ],
        out_specs=[
            pl.BlockSpec((tp, 1, rows, pc), lambda s: (0, s, 0, 0)),
            pl.BlockSpec((tp, 1, rows, qc), lambda s: (0, s, 0, 0)),
            per_seq(n_q, length),
        ],
        out_shape=[
            jax.ShapeDtypeStruct((tp, seqs, rows, pc), BF16),
            jax.ShapeDtypeStruct((tp, seqs, rows, qc), BF16),
            jax.ShapeDtypeStruct((seqs, n_q, length), F32),
        ],
        scratch_shapes=[
            pltpu.VMEM((n_kv, length + 2 * WINDOW, 128), BF16),
            pltpu.VMEM((n_q, length + 2 * WINDOW, 128), BF16),
            pltpu.VMEM((length + 128, pc), BF16),
            pltpu.VMEM((n_q, BLK, 3 * WINDOW), F32),
            pltpu.VMEM((groups, BLK, 2 * BLK), BF16),
        ],
        name="mixers",
    )(ints, floats, proj, kv_before, kv_after, pool_before, pool_after, pool_mix, q_gain, k_gain)

    pool_rows = lax.all_to_all(y_pool, "tp", split_axis=0, concat_axis=0, tiled=True)
    attn_rows = lax.all_to_all(y_attn, "tp", split_axis=0, concat_axis=0, tiled=True)

    mixed = pl.pallas_call(
        functools.partial(out_kernel, tp),
        grid=(seqs,),
        in_specs=[
            pl.BlockSpec((tp, 1, rows, pc), lambda s: (0, s, 0, 0)),
            pl.BlockSpec((tp, 1, rows, qc), lambda s: (0, s, 0, 0)),
            full(w_pool.shape), full(w_attn.shape),
        ],
        out_specs=per_seq(rows, model),
        out_shape=jax.ShapeDtypeStruct((seqs, rows, model), BF16),
        name="outproj",
    )(pool_rows, attn_rows, w_pool, w_attn)
    return jnp.transpose(mixed, (1, 0, 2)), jnp.transpose(lse, (2, 0, 1))


def solution(mesh):
    placed = (
        P("sp", None, None), P(), P(None, "tp"), P(None, "tp"), P("tp", None, None),
        P(None, "tp"), P(None, "tp"), P(None, "tp"), P(None, "tp"),
        P(), P(), P("tp"), P("sp", None), P("sp", None),
    )
    return jax.shard_map(
        body,
        mesh=mesh,
        in_specs=placed,
        out_specs=(P(("sp", "tp"), None, None), P("sp", None, "tp")),
        check_vma=False,
    )
```

profile of v0, /device:TPU:5, one launch (start us, length us, event | category | flops | bytes accessed | tf_op | source)
XLA Modules:
  0.0 217.3 jit_solution(4214527003691776194)
XLA Ops:
  7.2 0.0 all-gather.3.cloned.1.call-start
  7.2 0.7 all-gather.3.cloned.1.call-update
  7.9 0.0 all-gather.5.cloned.1.call-start
  7.9 0.7 all-gather.5.cloned.1.call-update
  8.6 2.4 %constant_dynamic-update-slice_fusion.5 = bf16[2048,1280]{1,0:T(8,128)(2,1)} fusion(bf16[2048,256]{1,0:T(8,128)(2,1)} %param.16), kind=kLoop, calls=%fused_computation.13 | loop fusion | bytes 2097152
  11.1 11.4 %multiply_reduce_fusion = f32[1024,4]{1,0:T(8,128)S(1)} fusion(bf16[1024,4,2048]{2,1,0:T(4,128)(2,1)} %param.14), kind=kLoop, calls=%fused_computation | loop fusion | flops 25161728 | bytes 16793600 | tf_op jit(solution)/shard_map/reduce_sum | solution.py:178
  22.4 0.0 copy-start.11
  22.4 0.1 add_rsqrt_fusion
  22.5 0.2 copy.24
  22.7 0.0 copy-done.2
  22.7 1.2 constant_dynamic-update-slice_fusion.4
  23.9 0.0 copy-done.3
  23.9 1.1 constant_dynamic-update-slice_fusion.3
  25.1 2.3 %constant_dynamic-update-slice_fusion.2 = bf16[2048,1280]{1,0:T(8,128)(2,1)} fusion(bf16[2048,1280]{1,0:T(8,128)(2,1)} %constant_dynamic-update-slice_fusion.3, bf16[2048,256]{1,0:T(8,128)(2,1)} %param.22), kind=kLoop, calls=%fused_computation.10 | loop fusion | bytes 2097152
  27.4 0.0 copy-done.4
  27.4 0.9 constant_dynamic-update-slice_fusion.1
  28.2 0.0 copy-done.5
  28.2 0.9 constant_dynamic-update-slice_fusion
  29.1 0.0 copy-done.11
  29.1 44.9 %fusion.proj = bf16[4,1024,1280]{2,1,0:T(8,128)(2,1)S(1)} fusion(bf16[1024,4,2048]{2,1,0:T(4,128)(2,1)} %param.14, f32[4,1024]{1,0:T(4,128)S(1)} %bitcast.15, bf16[2048,1280]{1,0:T(8,128)(2,1)} %constant_dynamic-update-slice_fusion, f32[2048]{0:T(1024)S(1)} %copy-done.11), kind=kOutput, calls=%fused_computation.2 | convolution fusion | flops 21493186560 | bytes 32530432 | tf_op jit(solution)/shard_map/tsd,dc->stc/dot_general | solution.py:183
  74.1 0.0 copy-start
  74.1 3.2 %collective-permute-start = (bf16[4,128,256]{2,1,0:T(8,128)(2,1)S(1)}, bf16[4,128,256]{2,1,0:T(8,128)(2,1)S(1)}, u32[]{:S(2)}, u32[]{:S(2)}) collective-permute-start(bf16[4,128,256]{2,1,0:T(8,128)(2,1)S(1)} %get-tuple-element.17), channel_id=1, source_target_pairs={{0,4},{4,8},{8,12},{12,16},{16,20},{20,24},{24,28},{1,5},{5,9},{9,... | collective-permute-start | bytes 786440 | tf_op jit(solution)/shard_map/ppermute | solution.py:27
  77.3 2.1 collective-permute-start.1
  79.4 0.0 copy-done
  79.5 4.0 %collective-permute-start.2 = (bf16[4,16,256]{2,1,0:T(8,128)(2,1)S(1)}, bf16[4,16,256]{2,1,0:T(8,128)(2,1)S(1)}, u32[]{:S(2)}, u32[]{:S(2)}) collective-permute-start(bf16[4,16,256]{2,1,0:T(8,128)(2,1)S(1)} %get-tuple-element.15), channel_id=1, source_target_pairs={{0,4},{4,8},{8,12},{12,16},{16,20},{20,24},{24,28},{1,5},{5,9},{9,... | collective-permute-start | bytes 98312 | tf_op jit(solution)/shard_map/ppermute | solution.py:27
  83.5 1.9 collective-permute-start.3
  85.5 0.0 copy-done.10
  85.5 0.0 copy-done.12
  85.5 0.6 pad_maximum_fusion.floats
  86.1 0.6 pad_add_fusion.ints
  86.8 0.7 broadcast_in_dim_tile.6.q_gain
  87.4 0.0 copy-done.13
  87.4 0.7 broadcast_in_dim_tile.7.k_gain
  88.1 2.2 %collective-permute-done.2.pool_before = bf16[4,16,256]{2,1,0:T(8,128)(2,1)S(1)} collective-permute-done((bf16[4,16,256]{2,1,0:T(8,128)(2,1)S(1)}, bf16[4,16,256]{2,1,0:T(8,128)(2,1)S(1)}, u32[]{:S(2)}, u32[]{:S(2)}) %collective-permute-start.2) | collective-permute-done | bytes 32800 | tf_op jit(solution)/shard_map/ppermute | solution.py:27
  90.3 0.0 collective-permute-done.3.pool_after
  90.3 0.0 collective-permute-done.kv_before
  90.3 0.0 copy-start.6
  90.3 0.0 collective-permute-done.1.kv_after
  90.3 0.6 copy-done.8
  90.9 0.0 copy-done.9
  90.9 0.1 copy-done.6
  91.1 0.7 copy-done.7
  91.8 37.3 %mixers.1 = (bf16[4,4,256,256]{3,2,1,0:T(8,128)(2,1)}, bf16[4,4,256,256]{3,2,1,0:T(8,128)(2,1)}, f32[4,4,1024]{2,1,0:T(4,128)}) custom-call(s32[3]{0:T(128)} %pad_add_fusion.ints, f32[3,4]{1,0:T(4,128)} %pad_maximum_fusion.floats, bf16[4,1024,1280]{2,1,0:T(8,128)(2,1)} %copy-done, bf16[4,128,256]{2,1,0:T(8,128)(2,1)} %copy-done.6, ...), custom_call_target="tpu_custom_call" | custom-call | tf_op jit(solution)/shard_map/mixers/pallas_call | solution.py:202
  129.1 30.8 %all_to_all.10.pool_rows = bf16[4,4,256,256]{3,2,1,0:T(8,128)(2,1)} all-to-all(bf16[4,4,256,256]{3,2,1,0:T(8,128)(2,1)} %get-tuple-element.5), channel_id=1, replica_groups=mesh['sp'=8,'tp'=4] {'tp'}, dimensions={0} | all-to-all | bytes 4194304 | tf_op jit(solution)/shard_map/all_to_all | solution.py:232
  159.9 0.0 copy-done.1
  159.9 28.9 %all_to_all.11.attn_rows = bf16[4,4,256,256]{3,2,1,0:T(8,128)(2,1)} all-to-all(bf16[4,4,256,256]{3,2,1,0:T(8,128)(2,1)S(1)} %copy-done.1), channel_id=1, replica_groups=mesh['sp'=8,'tp'=4] {'tp'}, dimensions={0} | all-to-all | bytes 4194304 | tf_op jit(solution)/shard_map/all_to_all | solution.py:233
  188.8 14.2 %outproj.1 = bf16[4,256,2048]{2,1,0:T(8,128)(2,1)} custom-call(bf16[4,4,256,256]{3,2,1,0:T(8,128)(2,1)} %all_to_all.10.pool_rows, bf16[4,4,256,256]{3,2,1,0:T(8,128)(2,1)} %all_to_all.11.attn_rows, bf16[1024,2048]{1,0:T(8,128)(2,1)} %all-gather.3.cloned.1.call-done.w_pool, bf16[1024,2048]{1,0:T(8,128)(2,1)} %all-gather.5.cloned.1.call-done.w_attn), custom_call_target="tpu_custom_call" | custom-call | tf_op jit(solution)/shard_map/outproj/pallas_call | solution.py:235
  203.0 7.4 %copy.23 = bf16[256,4,2048]{2,1,0:T(4,128)(2,1)} copy(bf16[256,4,2048]{2,0,1:T(8,128)(2,1)} %bitcast.14) | data formatting | bytes 8388608
  (21 shorter events, 0.1 us)
Async XLA Ops:
  7.2 181.7 %all-gather.3.cloned.1.call-start = ((), (), s32[]{:S(2)}) async-start(), calls=%async_computation.2 | async-start | bytes 4718592 | tf_op jit(solution)/shard_map/all_gather | solution.py:174
  7.9 181.0 %all-gather.5.cloned.1.call-start = ((), (), s32[]{:S(2)}) async-start(), calls=%async_computation.3 | async-start | bytes 4718592 | tf_op jit(solution)/shard_map/all_gather | solution.py:175
  11.1 11.7 %copy-start.2 = (bf16[2048,256]{1,0:T(8,128)(2,1)S(1)}, bf16[2048,256]{1,0:T(8,128)(2,1)}, u32[]{:S(2)}) copy-start(bf16[2048,256]{1,0:T(8,128)(2,1)} %param.17) | copy-start | bytes 3145732
  11.1 12.9 %copy-start.3 = (bf16[2048,256]{1,0:T(8,128)(2,1)S(1)}, bf16[2048,256]{1,0:T(8,128)(2,1)}, u32[]{:S(2)}) copy-start(bf16[2048,256]{1,0:T(8,128)(2,1)} %param.19) | copy-start | bytes 3145732
  22.4 4.9 %copy-start.4 = (bf16[2048,128]{1,0:T(8,128)(2,1)S(1)}, bf16[2048,128]{1,0:T(8,128)(2,1)}, u32[]{:S(2)}) copy-start(bf16[2048,128]{1,0:T(8,128)(2,1)} %param.20) | copy-start | bytes 1572868
  22.4 6.7 %copy-start.11 = (f32[2048]{0:T(1024)S(1)}, f32[2048]{0:T(1024)}, u32[]{:S(2)}) copy-start(f32[2048]{0:T(1024)} %param.15) | copy-start | bytes 24580
  22.7 5.5 %copy-start.5 = (bf16[2048,128]{1,0:T(8,128)(2,1)S(1)}, bf16[2048,128]{1,0:T(8,128)(2,1)}, u32[]{:S(2)}) copy-start(bf16[2048,128]{1,0:T(8,128)(2,1)} %param.21) | copy-start | bytes 1572868
  29.1 56.3 %copy-start.10 = (f32[4]{0:T(128)S(1)}, f32[4]{0:T(128)}, u32[]{:S(2)}) copy-start(f32[4]{0:T(128)} %param.25) | copy-start | bytes 52
  29.1 56.4 %copy-start.12 = (f32[64]{0:T(128)S(1)}, f32[64]{0:T(128)}, u32[]{:S(2)}) copy-start(f32[64]{0:T(128)} %param.23) | copy-start | bytes 772
  29.1 58.3 %copy-start.13 = (f32[64]{0:T(128)S(1)}, f32[64]{0:T(128)}, u32[]{:S(2)}) copy-start(f32[64]{0:T(128)} %param.24) | copy-start | bytes 772
  74.1 5.4 %copy-start = (bf16[4,1024,1280]{2,1,0:T(8,128)(2,1)}, bf16[4,1024,1280]{2,1,0:T(8,128)(2,1)S(1)}, u32[]{:S(2)}) copy-start(bf16[4,1024,1280]{2,1,0:T(8,128)(2,1)S(1)} %fusion.proj) | copy-start | bytes 31457284
  74.1 16.2 %collective-permute-start = (bf16[4,128,256]{2,1,0:T(8,128)(2,1)S(1)}, bf16[4,128,256]{2,1,0:T(8,128)(2,1)S(1)}, u32[]{:S(2)}, u32[]{:S(2)}) collective-permute-start(bf16[4,128,256]{2,1,0:T(8,128)(2,1)S(1)} %get-tuple-element.17), channel_id=1, source_target_pairs={{0,4},{4,8},{8,12},{12,16},{16,20},{20,24},{24,28},{1,5},{5,9},{9,... | collective-permute-start | bytes 786440 | tf_op jit(solution)/shard_map/ppermute | solution.py:27
  77.3 13.1 %collective-permute-start.1 = (bf16[4,128,256]{2,1,0:T(8,128)(2,1)S(1)}, bf16[4,128,256]{2,1,0:T(8,128)(2,1)S(1)}, u32[]{:S(2)}, u32[]{:S(2)}) collective-permute-start(bf16[4,128,256]{2,1,0:T(8,128)(2,1)S(1)} %get-tuple-element.16), channel_id=1, source_target_pairs={{4,0},{8,4},{12,8},{16,12},{20,16},{24,20},{28,24},{5,1},{9,5},{13... | collective-permute-start | bytes 786440 | tf_op jit(solution)/shard_map/ppermute | solution.py:28
  79.5 10.8 %collective-permute-start.2 = (bf16[4,16,256]{2,1,0:T(8,128)(2,1)S(1)}, bf16[4,16,256]{2,1,0:T(8,128)(2,1)S(1)}, u32[]{:S(2)}, u32[]{:S(2)}) collective-permute-start(bf16[4,16,256]{2,1,0:T(8,128)(2,1)S(1)} %get-tuple-element.15), channel_id=1, source_target_pairs={{0,4},{4,8},{8,12},{12,16},{16,20},{20,24},{24,28},{1,5},{5,9},{9,... | collective-permute-start | bytes 98312 | tf_op jit(solution)/shard_map/ppermute | solution.py:27
  83.5 6.8 %collective-permute-start.3 = (bf16[4,16,256]{2,1,0:T(8,128)(2,1)S(1)}, bf16[4,16,256]{2,1,0:T(8,128)(2,1)S(1)}, u32[]{:S(2)}, u32[]{:S(2)}) collective-permute-start(bf16[4,16,256]{2,1,0:T(8,128)(2,1)S(1)} %get-tuple-element.14), channel_id=1, source_target_pairs={{4,0},{8,4},{12,8},{16,12},{20,16},{24,20},{28,24},{5,1},{9,5},{13... | collective-permute-start | bytes 98312 | tf_op jit(solution)/shard_map/ppermute | solution.py:28
  90.3 0.6 copy-start.8
  90.3 0.6 copy-start.9
  90.3 0.7 copy-start.6
  91.1 0.7 copy-start.7
  129.1 30.8 %copy-start.1 = (bf16[4,4,256,256]{3,2,1,0:T(8,128)(2,1)S(1)}, bf16[4,4,256,256]{3,2,1,0:T(8,128)(2,1)}, u32[]{:S(2)}) copy-start(bf16[4,4,256,256]{3,2,1,0:T(8,128)(2,1)} %get-tuple-element.6) | copy-start | bytes 6291460
Sparse Core Ops, SparseCore 0:
  10.1 71.8 all-gather.2
  84.1 72.7 all-gather.4
where the time goes:
time: 221 us; the launch traced here: 217 us
  blocking collectives  59.7 us (27%)
  Pallas kernels  51.5 us (23%)
  matrix products  44.9 us (20%)
  local copies, waits for them, and re-layouts  19.3 us (9%)
  between operations  14.2 us (6%)
  other arithmetic  12.7 us (6%)
  starting transfers between devices  11.3 us (5%)
  waiting for transfers between devices  3.62 us (2%)
    dot_general x1, matrix products, body(): jnp.einsum('tsd,dc->stc', inputs, weights, preferred_element_type=F32)  44.9 us
    pallas_call x1, Pallas kernels, body(): pl.pallas_call(functools.partial(mix_kernel, pc, qc, kc, total_len), grid...  37.3 us
    all_to_all x1, blocking collectives, body(): lax.all_to_all(y_pool, 'tp', split_axis=0, concat_axis=0, tiled=True)  30.8 us
    all_to_all x1, blocking collectives, body(): lax.all_to_all(y_attn, 'tp', split_axis=0, concat_axis=0, tiled=True)  28.9 us
    unnamed x35, local copies, waits for them, and re-layouts  17 us
    pallas_call x1, Pallas kernels, body(): pl.pallas_call(functools.partial(out_kernel, tp), grid=(seqs,), in_specs=...  14.2 us
    reduce_sum x1, other arithmetic, body(): scale = lax.rsqrt(jnp.mean(flt * flt, axis=-1) + EPS)  11.4 us
    ppermute x2, starting transfers between devices, halo(): before = lax.ppermute(shard[:, length - width:], 'sp', up)  7.19 us
  transfers between devices with their start and end apart: 6, of which 1 were waited for; matrix products, arithmetic and copies ran while one was open for 31% of the time, Pallas kernels for 17%

commit v1 on v0

v1 whole, which is shorter than its diff:
```python
import functools
import math

import jax
import jax.numpy as jnp
from jax import lax
from jax.experimental import pallas as pl
from jax.experimental.pallas import tpu as pltpu
from jax.sharding import PartitionSpec as P

HEADS = 16
HEAD_DIM = 64
WINDOW = 128
EPS = 1e-06
NEG = -1e30
LOG2E = math.log2(math.e)
REACH = 16
BLK = 128
F32 = jnp.float32
BF16 = jnp.bfloat16
MESH = pl.DeviceIdType.MESH


def head_ones(cols):
    a = lax.broadcasted_iota(jnp.int32, (cols, cols), 0) // HEAD_DIM
    b = lax.broadcasted_iota(jnp.int32, (cols, cols), 1) // HEAD_DIM
    return jnp.where(a == b, 1.0 / HEAD_DIM, 0.0).astype(BF16)


def head_norm(values, gain):
    flt = values.astype(F32)
    mean = jnp.dot((flt * flt).astype(BF16), head_ones(flt.shape[-1]), preferred_element_type=F32)
    return (flt * lax.rsqrt(mean + EPS) * gain).astype(BF16)


def silu(gate):
    flt = gate.astype(F32)
    return flt / (1.0 + jnp.exp(-flt))


def mix_kernel(
    pc, qc, kc, count, tp, seqs, length, total_len,
    floats, proj, proj_any, w_any, mix, q_gain, k_gain,
    out, lse,
    keys, vals, pool_pad, bias, band, kv_halo, pool_halo, y_buf, y_recv, w_buf,
    halo_send, halo_recv, y_send, y_got, y_local, w_sems,
):
    rows = length // tp
    n_kv = kc // HEAD_DIM
    n_q = qc // HEAD_DIM
    groups = mix.shape[0]
    chan = mix.shape[1]
    i = pl.program_id(0)
    sp_me, me = lax.axis_index("sp"), lax.axis_index("tp")
    offset = sp_me * length
    half_widths = [jnp.left_shift(jnp.int32(1), (me * groups + g) % 4) for g in range(groups)]
    c_gate, c_q, c_ag, c_kv = pc, 2 * pc, 2 * pc + qc, 2 * pc + 2 * qc
    half_pad = 64
    core = me % 2
    sibling = me + 1 - 2 * core
    after = (sp_me + 1) % count
    before = (sp_me + count - 1) % count
    peers = [(me + d) % tp for d in range(1, tp)]

    def halo_copies(s):
        made = []
        for side, (target, first) in enumerate(((after, True), (before, False))):
            for kind, (buf, width, col, cols) in enumerate(
                ((kv_halo, WINDOW, c_kv, 2 * kc), (pool_halo, REACH, 0, pc))
            ):
                start = length - width if first else 0
                made.append(
                    pltpu.make_async_remote_copy(
                        src_ref=proj_any.at[s, pl.ds(start, width), pl.ds(col, cols)],
                        dst_ref=buf.at[side, s],
                        send_sem=halo_send.at[side, kind, s],
                        recv_sem=halo_recv.at[side, kind, s],
                        device_id={"sp": target},
                        device_id_type=MESH,
                    )
                )
        return made

    def y_copies(s):
        return [
            pltpu.make_async_remote_copy(
                src_ref=y_buf.at[s, peer],
                dst_ref=y_recv.at[me, s],
                send_sem=y_send.at[d, s],
                recv_sem=y_got.at[d, s],
                device_id={"tp": peer},
                device_id_type=MESH,
            )
            for d, peer in enumerate(peers)
        ]

    def y_own(s):
        return pltpu.make_async_copy(y_buf.at[s, me], y_recv.at[me, s], y_local.at[s])

    def w_copies():
        return (
            pltpu.make_async_remote_copy(
                src_ref=w_any, dst_ref=w_buf.at[core], send_sem=w_sems.at[0], recv_sem=w_sems.at[1],
                device_id={"tp": sibling}, device_id_type=MESH,
            ),
            pltpu.make_async_copy(w_any, w_buf.at[core], w_sems.at[2]),
        )

    @pl.when(i == 0)
    def _():
        barrier = pltpu.get_barrier_semaphore()
        for target in (after, before):
            pl.semaphore_signal(barrier, inc=1, device_id={"sp": target}, device_id_type=MESH)
        for peer in peers:
            pl.semaphore_signal(barrier, inc=1, device_id={"tp": peer}, device_id_type=MESH)
        pl.semaphore_wait(barrier, 2 + len(peers))
        for s in range(seqs):
            for copy in halo_copies(s):
                copy.start()
        for copy in w_copies():
            copy.start()
        ii = lax.broadcasted_iota(jnp.int32, (BLK, 3 * WINDOW), 0)
        jj = lax.broadcasted_iota(jnp.int32, (BLK, 3 * WINDOW), 1) - WINDOW
        dist = jnp.abs(ii - jj)
        for h in range(n_q):
            value = -floats[0, h] * dist.astype(F32) - floats[1, h]
            bias[h] = jnp.where(dist <= WINDOW, value, NEG)
        ti = lax.broadcasted_iota(jnp.int32, (BLK, 2 * BLK), 0)
        tj = lax.broadcasted_iota(jnp.int32, (BLK, 2 * BLK), 1) - half_pad
        rel = tj - ti
        for g in range(groups):
            hw = half_widths[g]
            inside = (rel >= -hw) & (rel <= hw - 1)
            band[g] = jnp.where(inside, 1.0, 0.0).astype(BF16)
        edge = jnp.zeros((half_pad - REACH, pc), BF16)
        pool_pad[0 : half_pad - REACH] = edge
        pool_pad[half_pad + length + REACH :] = edge

    def fill(first, size, kv):
        normed = head_norm(kv[:, :kc], k_gain[...])
        pos = lax.broadcasted_iota(jnp.int32, (size, HEAD_DIM), 0) + (offset + first - WINDOW)
        valid = (pos >= 0) & (pos < total_len)
        ones = jnp.where(valid, 1.0, 0.0).astype(BF16)
        for p in range(n_kv):
            k = normed[:, p * HEAD_DIM : (p + 1) * HEAD_DIM]
            v = kv[:, kc + p * HEAD_DIM : kc + (p + 1) * HEAD_DIM] * ones
            keys[p, first : first + size] = jnp.concatenate([k, k], axis=1)
            vals[2 * p, first : first + size] = jnp.concatenate([v, ones], axis=1)
            vals[2 * p + 1, first : first + size] = jnp.concatenate([ones, v], axis=1)

    low = lax.broadcasted_iota(jnp.int32, (BLK, 2 * HEAD_DIM), 1) < HEAD_DIM

    def step(b, carry):
        start = pl.multiple_of(b * BLK, BLK)
        dest = start // rows
        row = pl.multiple_of(start % rows, BLK)
        here = pl.ds(start, BLK)
        gpos = offset + start + lax.broadcasted_iota(jnp.int32, (BLK, chan), 0)
        for g in range(groups):
            hw = half_widths[g]
            cols = slice(g * chan, (g + 1) * chan)
            window = jnp.dot(band[g], pool_pad[pl.ds(start, 2 * BLK), cols], preferred_element_type=F32)
            lo = jnp.maximum(gpos - hw, 0)
            hi = jnp.minimum(gpos + hw - 1, total_len - 1)
            live = (hi - lo + 1).astype(F32)
            pooled = (window / live - proj[0, here, cols].astype(F32)).astype(BF16)
            mixed = jnp.dot(pooled, mix[g], preferred_element_type=F32)
            gate = proj[0, here, c_gate + g * chan : c_gate + (g + 1) * chan]
            y_buf[i, dest, pl.ds(row, BLK), cols] = (mixed * silu(gate)).astype(BF16)
        queries = head_norm(proj[0, here, c_q : c_q + qc], q_gain[...])
        for p in range(n_kv):
            pair = queries[:, p * 128 : (p + 1) * 128]
            zero = jnp.zeros_like(pair)
            stacked = jnp.concatenate([jnp.where(low, pair, zero), jnp.where(low, zero, pair)], axis=0)
            span = pl.ds(start, 3 * WINDOW)
            scores = lax.dot_general(
                stacked, keys[p, span], (((1,), (1,)), ((), ())), preferred_element_type=F32
            )
            w0 = jnp.exp2(scores[:BLK] + bias[2 * p]).astype(BF16)
            w1 = jnp.exp2(scores[BLK:] + bias[2 * p + 1]).astype(BF16)
            o0 = jnp.dot(w0, vals[2 * p, span], preferred_element_type=F32)
            o1 = jnp.dot(w1, vals[2 * p + 1, span], preferred_element_type=F32)
            num = jnp.where(low, o0, o1)
            tot = jnp.where(low, o1, o0) + 1.0
            den = pltpu.roll(tot, HEAD_DIM, 1)
            gate = proj[0, here, c_ag + p * 128 : c_ag + (p + 1) * 128]
            y_buf[i, dest, pl.ds(row, BLK), pc + p * 128 : pc + (p + 1) * 128] = (
                num / den * silu(gate)
            ).astype(BF16)
            tt = jnp.transpose(tot)
            lse[0, 2 * p : 2 * p + 1, here] = floats[2, 2 * p] + jnp.log(tt[HEAD_DIM : HEAD_DIM + 1])
            lse[0, 2 * p + 1 : 2 * p + 2, here] = floats[2, 2 * p + 1] + jnp.log(tt[0:1])
        return carry

    @pl.when(i < seqs)
    def _():
        pool_pad[half_pad : half_pad + length] = proj[0, :, :pc]
        fill(WINDOW, length, proj[0, :, c_kv:])
        for copy in halo_copies(i):
            copy.wait()
        first = jnp.where(sp_me > 0, 1.0, 0.0).astype(BF16)
        last = jnp.where(sp_me < count - 1, 1.0, 0.0).astype(BF16)
        pool_pad[half_pad - REACH : half_pad] = pool_halo[0, i] * first
        pool_pad[half_pad + length : half_pad + length + REACH] = pool_halo[1, i] * last
        fill(0, WINDOW, kv_halo[0, i])
        fill(WINDOW + length, WINDOW, kv_halo[1, i])
        lax.fori_loop(0, length // BLK, step, 0)
        for copy in y_copies(i):
            copy.start()
        y_own(i).start()

    @pl.when(i == seqs)
    def _():
        for copy in w_copies():
            copy.wait()

    @pl.when(i >= seqs)
    def _():
        s = i - seqs
        for copy in y_copies(s):
            copy.wait()
        y_own(s).wait()
        half = out.shape[-1] // 2
        depth = w_buf.shape[1] * w_buf.shape[3]
        pool_rows = jnp.concatenate([y_recv[p, s, :, :pc] for p in range(tp)], axis=1)
        attn_rows = jnp.concatenate([y_recv[p, s, :, pc:] for p in range(tp)], axis=1)
        for h in range(2):
            acc = jnp.dot(pool_rows, w_buf[h, :, 0].reshape(depth, half), preferred_element_type=F32)
            acc = acc + jnp.dot(attn_rows, w_buf[h, :, 1].reshape(depth, half), preferred_element_type=F32)
            out[0, :, h * half : (h + 1) * half] = acc.astype(BF16)


def body(
    inputs, norm_gain, pool_proj, pool_gate_proj, pool_mix, query_proj, key_proj, value_proj,
    attn_gate_proj, query_gain, key_gain, sink_logit, out_pool, out_attn,
):
    length, seqs, model = inputs.shape
    tp = lax.axis_size("tp")
    tp_index = lax.axis_index("tp")
    count = lax.axis_size("sp")
    total_len = length * count
    pc, qc, kc = pool_proj.shape[1], query_proj.shape[1], key_proj.shape[1]
    width = 2 * pc + 2 * qc + 2 * kc
    n_q = qc // HEAD_DIM
    n_kv = kc // HEAD_DIM
    groups = pool_mix.shape[0]
    rows = length // tp

    half = model // 2
    w_half = jnp.stack([out_pool, out_attn])
    w_half = lax.dynamic_slice_in_dim(w_half, (tp_index % 2) * half, half, 2)
    w_half = lax.all_gather(w_half, "sp", axis=0)

    flt = inputs.astype(F32)
    scale = lax.rsqrt(jnp.mean(flt * flt, axis=-1) + EPS)
    weights = jnp.concatenate(
        [pool_proj, pool_gate_proj, query_proj, attn_gate_proj, key_proj, value_proj], axis=1
    )
    weights = (weights.astype(F32) * norm_gain[:, None]).astype(BF16)
    proj = jnp.einsum("tsd,dc->stc", inputs, weights, preferred_element_type=F32)
    proj = (proj * scale.T[:, :, None]).astype(BF16)

    head_ids = tp_index * n_q + jnp.arange(n_q, dtype=jnp.int32)
    slopes = 2.0 ** (-8.0 * (head_ids + 1).astype(F32) / HEADS)
    floats = jnp.stack([slopes * LOG2E, sink_logit * LOG2E, sink_logit])
    q_gain = jnp.tile(query_gain * (HEAD_DIM**-0.5 * LOG2E), n_q)[None]
    k_gain = jnp.tile(key_gain, n_kv)[None]

    smem = pl.BlockSpec(memory_space=pltpu.SMEM)
    full = lambda shape: pl.BlockSpec(shape, lambda s: (0,) * len(shape))
    anywhere = pl.BlockSpec(memory_space=pl.ANY)
    early = lambda *shape: pl.BlockSpec(
        (1,) + shape, lambda i: (jnp.minimum(i, seqs - 1),) + (0,) * len(shape)
    )
    late = lambda *shape: pl.BlockSpec(
        (1,) + shape, lambda i: (jnp.maximum(i - seqs, 0),) + (0,) * len(shape)
    )
    dma = lambda *shape: pltpu.SemaphoreType.DMA(shape)
    mixed, lse = pl.pallas_call(
        functools.partial(mix_kernel, pc, qc, kc, count, tp, seqs, length, total_len),
        grid=(2 * seqs,),
        in_specs=[
            smem, early(length, width), anywhere, anywhere,
            full(pool_mix.shape), full((1, qc)), full((1, kc)),
        ],
        out_specs=[late(rows, model), early(n_q, length)],
        out_shape=[
            jax.ShapeDtypeStruct((seqs, rows, model), BF16),
            jax.ShapeDtypeStruct((seqs, n_q, length), F32),
        ],
        scratch_shapes=[
            pltpu.VMEM((n_kv, length + 2 * WINDOW, 128), BF16),
            pltpu.VMEM((n_q, length + 2 * WINDOW, 128), BF16),
            pltpu.VMEM((length + 128, pc), BF16),
            pltpu.VMEM((n_q, BLK, 3 * WINDOW), F32),
            pltpu.VMEM((groups, BLK, 2 * BLK), BF16),
            pltpu.VMEM((2, seqs, WINDOW, 2 * kc), BF16),
            pltpu.VMEM((2, seqs, REACH, pc), BF16),
            pltpu.VMEM((seqs, tp, rows, pc + qc), BF16),
            pltpu.VMEM((tp, seqs, rows, pc + qc), BF16),
            pltpu.VMEM((2,) + w_half.shape, BF16),
            dma(2, 2, seqs), dma(2, 2, seqs),
            dma(tp - 1, seqs), dma(tp - 1, seqs), dma(seqs), dma(3),
        ],
        compiler_params=pltpu.CompilerParams(collective_id=0, has_side_effects=True),
        name="mixers",
    )(floats, proj, proj, w_half, pool_mix, q_gain, k_gain)
    return jnp.transpose(mixed, (1, 0, 2)), jnp.transpose(lse, (2, 0, 1))


def solution(mesh):
    placed = (
        P("sp", None, None), P(), P(None, "tp"), P(None, "tp"), P("tp", None, None),
        P(None, "tp"), P(None, "tp"), P(None, "tp"), P(None, "tp"),
        P(), P(), P("tp"), P("sp", None), P("sp", None),
    )
    return jax.shard_map(
        body,
        mesh=mesh,
        in_specs=placed,
        out_specs=(P(("sp", "tp"), None, None), P("sp", None, "tp")),
        check_vma=False,
    )
```

time: 221 us -> 172 us (0.78); the launches traced: 217 us -> 172 us
  blocking collectives: 59.7 us -> 0 us
  Pallas kernels: 51.5 us -> 74 us
  starting transfers between devices: 11.3 us -> 0.04 us
    all_to_all x2 -> x0, blocking collectives: 59.7 us -> none  [the longest x1 30.8 us: body(): lax.all_to_all(y_pool, 'tp', split_axis=0, concat_axis=0, tiled=True)]
    pallas_call x2 -> x1, Pallas kernels: 51.5 us -> 74 us  [body(): pl.pallas_call(functools.partial(mix_kernel, pc, qc, kc, count, tp, seqs,...]
    ppermute x4 -> x0, starting transfers between devices: 11.3 us -> none  [the longest x2 7.19 us: halo(): before = lax.ppermute(shard[:, length - width:], 'sp', up)]
    all_gather x2 -> x1, waiting for transfers between devices: 0.01 us -> 3.39 us  [body(): w_half = lax.all_gather(w_half, 'sp', axis=0)]
    ppermute x4 -> x0, waiting for transfers between devices: 2.24 us -> none  [the longest x2 2.24 us: halo(): before = lax.ppermute(shard[:, length - width:], 'sp', up)]
    unnamed x35 -> x24, local copies, waits for them, and re-layouts: 17 us -> 15.9 us
  transfers between devices with their start and end apart: 6 -> 1, of which waited for: 1 -> 1; matrix products, arithmetic and copies ran while one was open for 31% -> 41% of each run, Pallas kernels for 17% -> 0%
where the time goes in v1:
time: 172 us
  Pallas kernels  74 us (43%)
  matrix products  46.3 us (27%)
  local copies, waits for them, and re-layouts  19 us (11%)
  other arithmetic  14.6 us (8%)
  between operations  14.1 us (8%)
  waiting for transfers between devices  3.41 us (2%)
    pallas_call x1, Pallas kernels, body(): pl.pallas_call(functools.partial(mix_kernel, pc, qc, kc, count, tp, seqs,...  74 us
    dot_general x1, matrix products, body(): jnp.einsum('tsd,dc->stc', inputs, weights, preferred_element_type=F32)  46.3 us
    unnamed x24, local copies, waits for them, and re-layouts  15.9 us
    reduce_sum x1, other arithmetic, body(): scale = lax.rsqrt(jnp.mean(flt * flt, axis=-1) + EPS)  11.4 us
  transfers between devices with their start and end apart: 1, of which 1 were waited for; matrix products, arithmetic and copies ran while one was open for 41% of the time, Pallas kernels for 0%

profile of v1, /device:TPU:5, one launch (start us, length us, event | category | flops | bytes accessed | tf_op | source)
XLA Modules:
  0.0 171.6 jit_solution(17162882601827728179)
XLA Ops:
  7.2 0.0 all-gather.3.cloned.1.call-start
  7.2 1.9 %fusion.5 = bf16[2,128,1024]{2,1,0:T(8,128)(2,1)} fusion(s32[]{:T(128)S(6)} %select_n.11, bf16[1,128,2048]{2,1,0:T(8,128)(2,1)} %bitcast.18, bf16[1,128,2048]{2,1,0:T(8,128)(2,1)} %bitcast.19), kind=kLoop, calls=%fused_computation.9 | loop fusion | flops 1048576 | bytes 1572868 | tf_op jit(solution)/shard_map/stack | solution.py:250
  9.1 0.0 all-gather.3.cloned.1.call-update
  9.2 0.7 multiply_bitcast_fusion
  9.8 0.0 copy-start
  9.8 0.0 copy-start.6
  9.8 0.0 copy-start.7
  9.9 0.0 copy-start.1
  9.9 11.4 %multiply_reduce_fusion = f32[1024,4]{1,0:T(8,128)S(1)} fusion(bf16[1024,4,2048]{2,1,0:T(4,128)(2,1)} %param.14), kind=kLoop, calls=%fused_computation | loop fusion | flops 25161728 | bytes 16793600 | tf_op jit(solution)/shard_map/reduce_sum | solution.py:255
  21.2 0.1 add_rsqrt_fusion
  21.3 0.2 copy.33
  21.5 0.0 copy-done
  21.5 0.0 copy-start.2
  21.5 0.0 copy-start.4
  21.5 0.0 copy-start.5
  21.5 1.1 constant_dynamic-update-slice_fusion.5
  22.6 0.0 copy-done.6
  22.6 0.6 broadcast_in_dim_tile.6.q_gain
  23.2 0.0 copy-done.7
  23.2 0.6 broadcast_in_dim_tile.7.k_gain
  23.9 0.0 copy-done.1
  23.9 1.1 constant_dynamic-update-slice_fusion.4
  24.9 2.4 %constant_dynamic-update-slice_fusion.3 = bf16[2048,1280]{1,0:T(8,128)(2,1)} fusion(bf16[2048,1280]{1,0:T(8,128)(2,1)} %constant_dynamic-update-slice_fusion.4, bf16[2048,256]{1,0:T(8,128)(2,1)} %param.19), kind=kLoop, calls=%fused_computation.14 | loop fusion | bytes 2097152
  27.3 0.0 copy-done.2
  27.3 1.1 constant_dynamic-update-slice_fusion.2
  28.4 1.9 %constant_dynamic-update-slice_fusion.1 = bf16[2048,1280]{1,0:T(8,128)(2,1)} fusion(bf16[2048,1280]{1,0:T(8,128)(2,1)} %constant_dynamic-update-slice_fusion.2, bf16[2048,128]{1,0:T(8,128)(2,1)} %param.20), kind=kLoop, calls=%fused_computation.12 | loop fusion | bytes 1048576
  30.3 1.9 %constant_dynamic-update-slice_fusion = bf16[2048,1280]{1,0:T(8,128)(2,1)} fusion(bf16[2048,1280]{1,0:T(8,128)(2,1)} %constant_dynamic-update-slice_fusion.1, bf16[2048,128]{1,0:T(8,128)(2,1)} %param.21), kind=kLoop, calls=%fused_computation.11 | loop fusion | bytes 1048576 | tf_op jit(solution)/shard_map/concatenate | solution.py:256
  32.2 0.0 copy-done.4
  32.3 0.6 pad_maximum_fusion.floats
  32.8 0.0 copy-done.5
  32.8 46.3 %fusion.proj.proj_any = bf16[4,1024,1280]{2,1,0:T(8,128)(2,1)} fusion(bf16[1024,4,2048]{2,1,0:T(4,128)(2,1)} %param.14, f32[4,1024]{1,0:T(4,128)S(1)} %bitcast.21, bf16[2048,1280]{1,0:T(8,128)(2,1)} %constant_dynamic-update-slice_fusion, f32[2048]{0:T(1024)S(1)} %copy-done.5), kind=kOutput, calls=%fused_computation.2 | convolution fusion | flops 21493186560 | bytes 32530432 | tf_op jit(solution)/shard_map/tsd,dc->stc/dot_general | solution.py:260
  79.2 3.4 %all-gather.3.cloned.1.call-done = bf16[16,128,1024]{2,1,0:T(8,128)(2,1)} async-done(((bf16[2,128,1024]{2,1,0:T(8,128)(2,1)}), bf16[16,128,1024]{2,1,0:T(8,128)(2,1)}) %all-gather.3.cloned.1.call-update) | async-done | bytes 4194320 | tf_op jit(solution)/shard_map/all_gather | solution.py:252
  82.6 74.0 %mixers.1 = (bf16[4,256,2048]{2,1,0:T(8,128)(2,1)}, f32[4,4,1024]{2,1,0:T(4,128)}) custom-call(f32[3,4]{1,0:T(4,128)} %pad_maximum_fusion.floats, bf16[4,1024,1280]{2,1,0:T(8,128)(2,1)} %fusion.proj.proj_any, bf16[4,1024,1280]{2,1,0:T(8,128)(2,1)} %fusion.proj.proj_any, bf16[8,2,128,1024]{3,2,1,0:T(8,128)(2,1)} %bitcast.17, bf16[2,128,128]{2,1,0:T(8,128)(2,1)} %mix.1, ...), custom_call_target="tpu_custom_call" | custom-call | tf_op jit(solution)/shard_map/mixers/pallas_call | solution.py:279
  156.6 0.0 copy-start.3
  156.6 7.5 %copy.29 = bf16[256,4,2048]{2,1,0:T(4,128)(2,1)} copy(bf16[256,4,2048]{2,0,1:T(8,128)(2,1)} %bitcast.16) | data formatting | bytes 8388608
  164.1 0.0 copy-done.3
  164.1 0.6 copy.42
  (4 shorter events, 0.0 us)
Async XLA Ops:
  7.2 75.4 %all-gather.3.cloned.1.call-start = ((), (), s32[]{:S(2)}) async-start(), calls=%async_computation | async-start | bytes 4718592 | tf_op jit(solution)/shard_map/all_gather | solution.py:252
  9.8 11.7 %copy-start = (bf16[2048,256]{1,0:T(8,128)(2,1)S(1)}, bf16[2048,256]{1,0:T(8,128)(2,1)}, u32[]{:S(2)}) copy-start(bf16[2048,256]{1,0:T(8,128)(2,1)} %param.16) | copy-start | bytes 3145732
  9.8 12.8 %copy-start.6 = (f32[64]{0:T(128)S(1)}, f32[64]{0:T(128)}, u32[]{:S(2)}) copy-start(f32[64]{0:T(128)} %param.23) | copy-start | bytes 772
  9.8 13.4 %copy-start.7 = (f32[64]{0:T(128)S(1)}, f32[64]{0:T(128)}, u32[]{:S(2)}) copy-start(f32[64]{0:T(128)} %param.24) | copy-start | bytes 772
  9.9 14.0 %copy-start.1 = (bf16[2048,256]{1,0:T(8,128)(2,1)S(1)}, bf16[2048,256]{1,0:T(8,128)(2,1)}, u32[]{:S(2)}) copy-start(bf16[2048,256]{1,0:T(8,128)(2,1)} %param.17) | copy-start | bytes 3145732
  21.5 5.8 %copy-start.2 = (bf16[2048,256]{1,0:T(8,128)(2,1)S(1)}, bf16[2048,256]{1,0:T(8,128)(2,1)}, u32[]{:S(2)}) copy-start(bf16[2048,256]{1,0:T(8,128)(2,1)} %param.22) | copy-start | bytes 3145732
  21.5 10.8 %copy-start.4 = (f32[4]{0:T(128)S(1)}, f32[4]{0:T(128)}, u32[]{:S(2)}) copy-start(f32[4]{0:T(128)} %param.25) | copy-start | bytes 52
  21.5 11.3 %copy-start.5 = (f32[2048]{0:T(1024)S(1)}, f32[2048]{0:T(1024)}, u32[]{:S(2)}) copy-start(f32[2048]{0:T(1024)} %param.15) | copy-start | bytes 24580
  156.6 7.5 %copy-start.3 = (f32[4,4,1024]{2,1,0:T(4,128)S(1)}, f32[4,4,1024]{2,1,0:T(4,128)}, u32[]{:S(2)}) copy-start(f32[4,4,1024]{2,1,0:T(4,128)} %get-tuple-element.5) | copy-start | bytes 196612
Sparse Core Ops, SparseCore 0:
  10.7 71.8 all-gather.2

commit v2 on v1

--- a/solution.py
+++ b/solution.py
@@ -40,10 +40,10 @@
 
 def mix_kernel(
     pc, qc, kc, count, tp, seqs, length, total_len,
-    floats, proj, proj_any, w_any, mix, q_gain, k_gain,
-    out, lse,
-    keys, vals, pool_pad, bias, band, kv_halo, pool_halo, y_buf, y_recv, w_buf,
-    halo_send, halo_recv, y_send, y_got, y_local, w_sems,
+    floats, proj, proj_any, mix, q_gain, k_gain,
+    y_recv, lse,
+    keys, vals, pool_pad, bias, band, kv_halo, pool_halo, y_buf,
+    halo_send, halo_recv, y_send, y_got, y_local,
 ):
     rows = length // tp
     n_kv = kc // HEAD_DIM
@@ -56,8 +56,6 @@
     half_widths = [jnp.left_shift(jnp.int32(1), (me * groups + g) % 4) for g in range(groups)]
     c_gate, c_q, c_ag, c_kv = pc, 2 * pc, 2 * pc + qc, 2 * pc + 2 * qc
     half_pad = 64
-    core = me % 2
-    sibling = me + 1 - 2 * core
     after = (sp_me + 1) % count
     before = (sp_me + count - 1) % count
     peers = [(me + d) % tp for d in range(1, tp)]
@@ -97,15 +95,6 @@
     def y_own(s):
         return pltpu.make_async_copy(y_buf.at[s, me], y_recv.at[me, s], y_local.at[s])
 
-    def w_copies():
-        return (
-            pltpu.make_async_remote_copy(
-                src_ref=w_any, dst_ref=w_buf.at[core], send_sem=w_sems.at[0], recv_sem=w_sems.at[1],
-                device_id={"tp": sibling}, device_id_type=MESH,
-            ),
-            pltpu.make_async_copy(w_any, w_buf.at[core], w_sems.at[2]),
-        )
-
     @pl.when(i == 0)
     def _():
         barrier = pltpu.get_barrier_semaphore()
@@ -117,8 +106,6 @@
         for s in range(seqs):
             for copy in halo_copies(s):
                 copy.start()
-        for copy in w_copies():
-            copy.start()
         ii = lax.broadcasted_iota(jnp.int32, (BLK, 3 * WINDOW), 0)
         jj = lax.broadcasted_iota(jnp.int32, (BLK, 3 * WINDOW), 1) - WINDOW
         dist = jnp.abs(ii - jj)
@@ -192,42 +179,80 @@
             lse[0, 2 * p + 1 : 2 * p + 2, here] = floats[2, 2 * p + 1] + jnp.log(tt[0:1])
         return carry
 
-    @pl.when(i < seqs)
+    pool_pad[half_pad : half_pad + length] = proj[0, :, :pc]
+    fill(WINDOW, length, proj[0, :, c_kv:])
+    for copy in halo_copies(i):
+        copy.wait()
+    first = jnp.where(sp_me > 0, 1.0, 0.0).astype(BF16)
+    last = jnp.where(sp_me < count - 1, 1.0, 0.0).astype(BF16)
+    pool_pad[half_pad - REACH : half_pad] = pool_halo[0, i] * first
+    pool_pad[half_pad + length : half_pad + length + REACH] = pool_halo[1, i] * last
+    fill(0, WINDOW, kv_halo[0, i])
+    fill(WINDOW + length, WINDOW, kv_halo[1, i])
+    lax.fori_loop(0, length // BLK, step, 0)
+    for copy in y_copies(i):
+        copy.start()
+    y_own(i).start()
+
+    @pl.when(i == seqs - 1)
     def _():
-        pool_pad[half_pad : half_pad + length] = proj[0, :, :pc]
-        fill(WINDOW, length, proj[0, :, c_kv:])
-        for copy in halo_copies(i):
-            copy.wait()
-        first = jnp.where(sp_me > 0, 1.0, 0.0).astype(BF16)
-        last = jnp.where(sp_me < count - 1, 1.0, 0.0).astype(BF16)
-        pool_pad[half_pad - REACH : half_pad] = pool_halo[0, i] * first
-        pool_pad[half_pad + length : half_pad + length + REACH] = pool_halo[1, i] * last
-        fill(0, WINDOW, kv_halo[0, i])
-        fill(WINDOW + length, WINDOW, kv_halo[1, i])
-        lax.fori_loop(0, length // BLK, step, 0)
-        for copy in y_copies(i):
-            copy.start()
-        y_own(i).start()
+        for t in range(seqs):
+            for copy in y_copies(t):
+                copy.wait()
+            y_own(t).wait()
+
+
+def out_kernel(tp, seqs, pc, y_ref, w_any, out, w_buf, sems):
+    i = pl.program_id(0)
+    me = lax.axis_index("tp")
+    core = me % 2
+    sibling = me + 1 - 2 * core
+    local = pltpu.make_async_copy(w_any, w_buf.at[0], sems.at[2])
+    swap = pltpu.make_async_remote_copy(
+        src_ref=w_any, dst_ref=w_buf.at[1], send_sem=sems.at[0], recv_sem=sems.at[1],
+        device_id={"tp": sibling}, device_id_type=MESH,
+    )
+
+    @pl.when(i == 0)
+    def _():
+        barrier = pltpu.get_barrier_semaphore()
+        pl.semaphore_signal(barrier, inc=1, device_id={"tp": sibling}, device_id_type=MESH)
+        local.start()
+        pl.semaphore_wait(barrier, 1)
+        swap.start()
+        local.wait()
 
     @pl.when(i == seqs)
     def _():
-        for copy in w_copies():
-            copy.wait()
-
-    @pl.when(i >= seqs)
-    def _():
-        s = i - seqs
-        for copy in y_copies(s):
-            copy.wait()
-        y_own(s).wait()
-        half = out.shape[-1] // 2
-        depth = w_buf.shape[1] * w_buf.shape[3]
-        pool_rows = jnp.concatenate([y_recv[p, s, :, :pc] for p in range(tp)], axis=1)
-        attn_rows = jnp.concatenate([y_recv[p, s, :, pc:] for p in range(tp)], axis=1)
-        for h in range(2):
-            acc = jnp.dot(pool_rows, w_buf[h, :, 0].reshape(depth, half), preferred_element_type=F32)
-            acc = acc + jnp.dot(attn_rows, w_buf[h, :, 1].reshape(depth, half), preferred_element_type=F32)
-            out[0, :, h * half : (h + 1) * half] = acc.astype(BF16)
+        swap.wait()
+
+    h = i // seqs
+    half = out.shape[-1] // 2
+    depth = w_buf.shape[1] * w_buf.shape[3]
+    pool_rows = jnp.concatenate([y_ref[p, 0, :, :pc] for p in range(tp)], axis=1)
+    attn_rows = jnp.concatenate([y_ref[p, 0, :, pc:] for p in range(tp)], axis=1)
+    acc = jnp.dot(pool_rows, w_buf[h, :, 0].reshape(depth, half), preferred_element_type=F32)
+    acc = acc + jnp.dot(attn_rows, w_buf[h, :, 1].reshape(depth, half), preferred_element_type=F32)
+    col = pl.multiple_of(((core + h) % 2) * half, half)
+    out[i % seqs, :, pl.ds(col, half)] = acc.astype(BF16)
+
+
+def proj_kernel(x_ref, gain, *refs):
+    weights, out, wide = refs[:-2], refs[-2], refs[-1]
+    tile, seqs, model = x_ref.shape
+    flt = x_ref[...].reshape(tile * seqs, model).astype(F32)
+    mean = jnp.mean(flt * flt, axis=-1, keepdims=True)
+    hidden = (flt * lax.rsqrt(mean + EPS) * gain[...]).astype(BF16)
+    col = 0
+    for w in weights:
+        size = w.shape[1]
+        res = jnp.dot(hidden, w[...], preferred_element_type=F32)
+        for c in range(0, size, 128):
+            n = min(128, size - c)
+            wide[:, :n] = res[:, c : c + n]
+            for s in range(seqs):
+                out[s, :, col + c : col + c + n] = wide[pl.ds(s, tile, stride=seqs), :n].astype(BF16)
+        col += size
 
 
 def body(
@@ -251,14 +276,20 @@
     w_half = lax.dynamic_slice_in_dim(w_half, (tp_index % 2) * half, half, 2)
     w_half = lax.all_gather(w_half, "sp", axis=0)
 
-    flt = inputs.astype(F32)
-    scale = lax.rsqrt(jnp.mean(flt * flt, axis=-1) + EPS)
-    weights = jnp.concatenate(
-        [pool_proj, pool_gate_proj, query_proj, attn_gate_proj, key_proj, value_proj], axis=1
-    )
-    weights = (weights.astype(F32) * norm_gain[:, None]).astype(BF16)
-    proj = jnp.einsum("tsd,dc->stc", inputs, weights, preferred_element_type=F32)
-    proj = (proj * scale.T[:, :, None]).astype(BF16)
+    weights = [pool_proj, pool_gate_proj, query_proj, attn_gate_proj, key_proj, value_proj]
+    tile = BLK
+    proj = pl.pallas_call(
+        proj_kernel,
+        grid=(length // tile,),
+        in_specs=[
+            pl.BlockSpec((tile, seqs, model), lambda t: (t, 0, 0)),
+            pl.BlockSpec((1, model), lambda t: (0, 0)),
+        ] + [pl.BlockSpec(w.shape, lambda t: (0, 0)) for w in weights],
+        out_specs=pl.BlockSpec((seqs, tile, width), lambda t: (0, t, 0)),
+        out_shape=jax.ShapeDtypeStruct((seqs, length, width), BF16),
+        scratch_shapes=[pltpu.VMEM((tile * seqs, 128), F32)],
+        name="projections",
+    )(inputs, norm_gain[None], *weights)
 
     head_ids = tp_index * n_q + jnp.arange(n_q, dtype=jnp.int32)
     slopes = 2.0 ** (-8.0 * (head_ids + 1).astype(F32) / HEADS)
@@ -269,23 +300,18 @@
     smem = pl.BlockSpec(memory_space=pltpu.SMEM)
     full = lambda shape: pl.BlockSpec(shape, lambda s: (0,) * len(shape))
     anywhere = pl.BlockSpec(memory_space=pl.ANY)
-    early = lambda *shape: pl.BlockSpec(
-        (1,) + shape, lambda i: (jnp.minimum(i, seqs - 1),) + (0,) * len(shape)
-    )
-    late = lambda *shape: pl.BlockSpec(
-        (1,) + shape, lambda i: (jnp.maximum(i - seqs, 0),) + (0,) * len(shape)
-    )
+    per_seq = lambda *shape: pl.BlockSpec((1,) + shape, lambda i: (i,) + (0,) * len(shape))
     dma = lambda *shape: pltpu.SemaphoreType.DMA(shape)
-    mixed, lse = pl.pallas_call(
+    y_recv, lse = pl.pallas_call(
         functools.partial(mix_kernel, pc, qc, kc, count, tp, seqs, length, total_len),
-        grid=(2 * seqs,),
+        grid=(seqs,),
         in_specs=[
-            smem, early(length, width), anywhere, anywhere,
+            smem, per_seq(length, width), anywhere,
             full(pool_mix.shape), full((1, qc)), full((1, kc)),
         ],
-        out_specs=[late(rows, model), early(n_q, length)],
+        out_specs=[anywhere, per_seq(n_q, length)],
         out_shape=[
-            jax.ShapeDtypeStruct((seqs, rows, model), BF16),
+            jax.ShapeDtypeStruct((tp, seqs, rows, pc + qc), BF16),
             jax.ShapeDtypeStruct((seqs, n_q, length), F32),
         ],
         scratch_shapes=[
@@ -297,14 +323,25 @@
             pltpu.VMEM((2, seqs, WINDOW, 2 * kc), BF16),
             pltpu.VMEM((2, seqs, REACH, pc), BF16),
             pltpu.VMEM((seqs, tp, rows, pc + qc), BF16),
-            pltpu.VMEM((tp, seqs, rows, pc + qc), BF16),
-            pltpu.VMEM((2,) + w_half.shape, BF16),
             dma(2, 2, seqs), dma(2, 2, seqs),
-            dma(tp - 1, seqs), dma(tp - 1, seqs), dma(seqs), dma(3),
+            dma(tp - 1, seqs), dma(tp - 1, seqs), dma(seqs),
         ],
         compiler_params=pltpu.CompilerParams(collective_id=0, has_side_effects=True),
         name="mixers",
-    )(floats, proj, proj, w_half, pool_mix, q_gain, k_gain)
+    )(floats, proj, proj, pool_mix, q_gain, k_gain)
+
+    mixed = pl.pallas_call(
+        functools.partial(out_kernel, tp, seqs, pc),
+        grid=(2 * seqs,),
+        in_specs=[
+            pl.BlockSpec((tp, 1, rows, pc + qc), lambda i: (0, i % seqs, 0, 0)), anywhere,
+        ],
+        out_specs=full((seqs, rows, model)),
+        out_shape=jax.ShapeDtypeStruct((seqs, rows, model), BF16),
+        scratch_shapes=[pltpu.VMEM((2,) + w_half.shape, BF16), dma(3)],
+        compiler_params=pltpu.CompilerParams(collective_id=1, has_side_effects=True),
+        name="outproj",
+    )(y_recv, w_half)
     return jnp.transpose(mixed, (1, 0, 2)), jnp.transpose(lse, (2, 0, 1))
 
 

time: 172 us -> 150 us (0.87)
  Pallas kernels: 74 us -> 123 us
  matrix products: 46.3 us -> 0 us
  other arithmetic: 14.6 us -> 3.17 us
  local copies, waits for them, and re-layouts: 19 us -> 10.1 us
  waiting for transfers between devices: 3.41 us -> 0.04 us
    pallas_call x0 -> x2, Pallas kernels: none -> 53.8 us  [the longest x1 38 us: body(): pl.pallas_call(proj_kernel, grid=(length // tile,), in_specs=[pl.BlockSpe...]
    dot_general x1 -> x0, matrix products: 46.3 us -> none  [body(): jnp.einsum('tsd,dc->stc', inputs, weights, preferred_element_type=F32)]
    reduce_sum x1 -> x0, other arithmetic: 11.4 us -> none  [body(): scale = lax.rsqrt(jnp.mean(flt * flt, axis=-1) + EPS)]
    unnamed x24 -> x6, local copies, waits for them, and re-layouts: 15.9 us -> 8.11 us
    pallas_call x1, Pallas kernels: 74 us -> 68.9 us  [body(): pl.pallas_call(functools.partial(mix_kernel, pc, qc, kc, count, tp, seqs,...]
    all_gather x1, waiting for transfers between devices: 3.39 us -> 0.02 us  [body(): w_half = lax.all_gather(w_half, 'sp', axis=0)]
    concatenate x1 -> x0, local copies, waits for them, and re-layouts: 1.93 us -> none  [body(): jnp.concatenate([pool_proj, pool_gate_proj, query_proj, attn_gate_proj, k...]
  transfers between devices with their start and end apart: 1 -> 1, of which waited for: 1 -> 0; matrix products, arithmetic and copies ran while one was open for 41% -> 2% of each run, Pallas kernels for 0% -> 71%
where the time goes in v2:
time: 150 us
  Pallas kernels  123 us (82%)
  between operations  14.1 us (9%)
  local copies, waits for them, and re-layouts  10.1 us (7%)
  other arithmetic  3.17 us (2%)
    pallas_call x1, Pallas kernels, body(): pl.pallas_call(functools.partial(mix_kernel, pc, qc, kc, count, tp, seqs,...  68.9 us
    pallas_call x1, Pallas kernels, body(): pl.pallas_call(proj_kernel, grid=(length // tile,), in_specs=[pl.BlockSpe...  38 us
    pallas_call x1, Pallas kernels, body(): pl.pallas_call(functools.partial(out_kernel, tp, seqs, pc), grid=(2 * seq...  15.8 us
    unnamed x6, local copies, waits for them, and re-layouts  8.11 us
  transfers between devices with their start and end apart: 1, of which 0 were waited for; matrix products, arithmetic and copies ran while one was open for 2% of the time, Pallas kernels for 71%

profile of v2, /device:TPU:5, one launch (start us, length us, event | category | flops | bytes accessed | tf_op | source)
XLA Modules:
  0.0 150.0 jit_solution(18325875406070461471)
XLA Ops:
  7.2 0.0 all-gather.3.cloned.1.call-start
  7.2 1.9 %fusion = bf16[2,128,1024]{2,1,0:T(8,128)(2,1)} fusion(s32[]{:T(128)S(6)} %select_n.11, bf16[1,128,2048]{2,1,0:T(8,128)(2,1)} %bitcast.11, bf16[1,128,2048]{2,1,0:T(8,128)(2,1)} %bitcast.12), kind=kLoop, calls=%fused_computation.2 | loop fusion | flops 1048576 | bytes 1572868 | tf_op jit(solution)/shard_map/stack | solution.py:275
  9.1 0.0 all-gather.3.cloned.1.call-update
  9.2 0.7 broadcast_multiply_fusion
  9.8 0.7 broadcast_in_dim_tile.6.q_gain
  10.5 0.7 tile.5
  11.2 0.6 broadcast_in_dim_tile.7.k_gain
  11.8 0.0 copy-start.1
  11.8 38.0 %projections.1.proj.proj_any = bf16[4,1024,1280]{2,1,0:T(8,128)(2,1)} custom-call(bf16[1024,4,2048]{2,1,0:T(4,128)(2,1)} %x_ref.1, f32[1,2048]{1,0:T(1,128)} %bitcast.14, bf16[2048,256]{1,0:T(8,128)(2,1)} %refs_0_.1, bf16[2048,256]{1,0:T(8,128)(2,1)} %refs_1_.1, bf16[2048,256]{1,0:T(8,128)(2,1)} %refs_2_.1, bf16[2048,256]{1,0:T(8,128)(2,1)} %refs_3_.1, ...), custom_call_target="tpu_custom_call" | custom-call | tf_op jit(solution)/shard_map/projections/pallas_call | solution.py:281
  49.8 0.0 copy-done.1
  49.8 0.6 pad_maximum_fusion.floats
  50.4 68.9 %mixers.1 = (bf16[4,4,256,512]{3,2,1,0:T(8,128)(2,1)}, f32[4,4,1024]{2,1,0:T(4,128)}) custom-call(f32[3,4]{1,0:T(4,128)} %pad_maximum_fusion.floats, bf16[4,1024,1280]{2,1,0:T(8,128)(2,1)} %projections.1.proj.proj_any, bf16[4,1024,1280]{2,1,0:T(8,128)(2,1)} %projections.1.proj.proj_any, bf16[2,128,128]{2,1,0:T(8,128)(2,1)} %mix.1, ...), custom_call_target="tpu_custom_call" | custom-call | tf_op jit(solution)/shard_map/mixers/pallas_call | solution.py:305
  119.3 0.0 all-gather.3.cloned.1.call-done
  119.3 15.8 %outproj.1 = bf16[4,256,2048]{2,1,0:T(8,128)(2,1)} custom-call(bf16[4,4,256,512]{3,2,1,0:T(8,128)(2,1)} %get-tuple-element.4.y_ref, bf16[8,2,128,1024]{3,2,1,0:T(8,128)(2,1)} %bitcast.10), custom_call_target="tpu_custom_call" | custom-call | tf_op jit(solution)/shard_map/outproj/pallas_call | solution.py:333
  135.1 0.0 copy-start
  135.1 7.5 %copy.17 = bf16[256,4,2048]{2,1,0:T(4,128)(2,1)} copy(bf16[256,4,2048]{2,0,1:T(8,128)(2,1)} %bitcast.9) | data formatting | bytes 8388608
  142.6 0.0 copy-done
  142.6 0.6 copy.19
  (3 shorter events, 0.0 us)
Async XLA Ops:
  7.2 112.1 %all-gather.3.cloned.1.call-start = ((), (), s32[]{:S(2)}) async-start(), calls=%async_computation | async-start | bytes 4718592 | tf_op jit(solution)/shard_map/all_gather | solution.py:277
  11.8 38.0 %copy-start.1 = (f32[4]{0:T(128)S(1)}, f32[4]{0:T(128)}, u32[]{:S(2)}) copy-start(f32[4]{0:T(128)} %param.25) | copy-start | bytes 52
  135.1 7.5 %copy-start = (f32[4,4,1024]{2,1,0:T(4,128)S(1)}, f32[4,4,1024]{2,1,0:T(4,128)}, u32[]{:S(2)}) copy-start(f32[4,4,1024]{2,1,0:T(4,128)} %get-tuple-element.5) | copy-start | bytes 196612
Sparse Core Ops, SparseCore 0:
  10.7 84.8 all-gather.2

commit v3 on v2

--- a/solution.py
+++ b/solution.py
@@ -189,10 +189,10 @@
     pool_pad[half_pad + length : half_pad + length + REACH] = pool_halo[1, i] * last
     fill(0, WINDOW, kv_halo[0, i])
     fill(WINDOW + length, WINDOW, kv_halo[1, i])
-    lax.fori_loop(0, length // BLK, step, 0)
-    for copy in y_copies(i):
+    per = rows // BLK
+    for dest, copy in zip(peers + [me], y_copies(i) + [y_own(i)]):
+        lax.fori_loop(0, per, lambda b, c, dest=dest: step(dest * per + b, c), 0)
         copy.start()
-    y_own(i).start()
 
     @pl.when(i == seqs - 1)
     def _():

time: 150 us -> 144 us (0.960)
  Pallas kernels: 123 us -> 117 us
    pallas_call x1, Pallas kernels: 68.9 us -> 62.9 us  [body(): pl.pallas_call(functools.partial(mix_kernel, pc, qc, kc, count, tp, seqs,...]
  transfers between devices with their start and end apart: 1 -> 1, of which waited for: 0 -> 0; matrix products, arithmetic and copies ran while one was open for 2% -> 2% of each run, Pallas kernels for 71% -> 70%
where the time goes in v3:
time: 144 us
  Pallas kernels  117 us (81%)
  between operations  14.1 us (10%)
  local copies, waits for them, and re-layouts  10.1 us (7%)
  other arithmetic  3.17 us (2%)
    pallas_call x1, Pallas kernels, body(): pl.pallas_call(functools.partial(mix_kernel, pc, qc, kc, count, tp, seqs,...  62.9 us
    pallas_call x1, Pallas kernels, body(): pl.pallas_call(proj_kernel, grid=(length // tile,), in_specs=[pl.BlockSpe...  38 us
    pallas_call x1, Pallas kernels, body(): pl.pallas_call(functools.partial(out_kernel, tp, seqs, pc), grid=(2 * seq...  15.7 us
    unnamed x6, local copies, waits for them, and re-layouts  8.11 us
  transfers between devices with their start and end apart: 1, of which 0 were waited for; matrix products, arithmetic and copies ran while one was open for 2% of the time, Pallas kernels for 70%

profile of v3, /device:TPU:5, one launch (start us, length us, event | category | flops | bytes accessed | tf_op | source)
XLA Modules:
  0.0 144.1 jit_solution(8755756673185046767)
XLA Ops:
  7.2 0.0 all-gather.3.cloned.1.call-start
  7.2 1.9 %fusion = bf16[2,128,1024]{2,1,0:T(8,128)(2,1)} fusion(s32[]{:T(128)S(6)} %select_n.11, bf16[1,128,2048]{2,1,0:T(8,128)(2,1)} %bitcast.11, bf16[1,128,2048]{2,1,0:T(8,128)(2,1)} %bitcast.12), kind=kLoop, calls=%fused_computation.2 | loop fusion | flops 1048576 | bytes 1572868 | tf_op jit(solution)/shard_map/stack | solution.py:275
  9.1 0.0 all-gather.3.cloned.1.call-update
  9.2 0.7 broadcast_multiply_fusion
  9.8 0.7 broadcast_in_dim_tile.6.q_gain
  10.5 0.7 tile.5
  11.2 0.6 broadcast_in_dim_tile.7.k_gain
  11.8 0.0 copy-start.1
  11.8 38.0 %projections.1.proj.proj_any = bf16[4,1024,1280]{2,1,0:T(8,128)(2,1)} custom-call(bf16[1024,4,2048]{2,1,0:T(4,128)(2,1)} %x_ref.1, f32[1,2048]{1,0:T(1,128)} %bitcast.14, bf16[2048,256]{1,0:T(8,128)(2,1)} %refs_0_.1, bf16[2048,256]{1,0:T(8,128)(2,1)} %refs_1_.1, bf16[2048,256]{1,0:T(8,128)(2,1)} %refs_2_.1, bf16[2048,256]{1,0:T(8,128)(2,1)} %refs_3_.1, ...), custom_call_target="tpu_custom_call" | custom-call | tf_op jit(solution)/shard_map/projections/pallas_call | solution.py:281
  49.8 0.0 copy-done.1
  49.8 0.6 pad_maximum_fusion.floats
  50.4 62.9 %mixers.1 = (bf16[4,4,256,512]{3,2,1,0:T(8,128)(2,1)}, f32[4,4,1024]{2,1,0:T(4,128)}) custom-call(f32[3,4]{1,0:T(4,128)} %pad_maximum_fusion.floats, bf16[4,1024,1280]{2,1,0:T(8,128)(2,1)} %projections.1.proj.proj_any, bf16[4,1024,1280]{2,1,0:T(8,128)(2,1)} %projections.1.proj.proj_any, bf16[2,128,128]{2,1,0:T(8,128)(2,1)} %mix.1, ...), custom_call_target="tpu_custom_call" | custom-call | tf_op jit(solution)/shard_map/mixers/pallas_call | solution.py:305
  113.4 0.0 all-gather.3.cloned.1.call-done
  113.4 15.7 %outproj.1 = bf16[4,256,2048]{2,1,0:T(8,128)(2,1)} custom-call(bf16[4,4,256,512]{3,2,1,0:T(8,128)(2,1)} %get-tuple-element.4.y_ref, bf16[8,2,128,1024]{3,2,1,0:T(8,128)(2,1)} %bitcast.10), custom_call_target="tpu_custom_call" | custom-call | tf_op jit(solution)/shard_map/outproj/pallas_call | solution.py:333
  129.2 0.0 copy-start
  129.2 7.5 %copy.17 = bf16[256,4,2048]{2,1,0:T(4,128)(2,1)} copy(bf16[256,4,2048]{2,0,1:T(8,128)(2,1)} %bitcast.9) | data formatting | bytes 8388608
  136.6 0.0 copy-done
  136.6 0.6 copy.19
  (3 shorter events, 0.0 us)
Async XLA Ops:
  7.2 106.2 %all-gather.3.cloned.1.call-start = ((), (), s32[]{:S(2)}) async-start(), calls=%async_computation | async-start | bytes 4718592 | tf_op jit(solution)/shard_map/all_gather | solution.py:277
  11.8 38.0 %copy-start.1 = (f32[4]{0:T(128)S(1)}, f32[4]{0:T(128)}, u32[]{:S(2)}) copy-start(f32[4]{0:T(128)} %param.25) | copy-start | bytes 52
  129.2 7.5 %copy-start = (f32[4,4,1024]{2,1,0:T(4,128)S(1)}, f32[4,4,1024]{2,1,0:T(4,128)}, u32[]{:S(2)}) copy-start(f32[4,4,1024]{2,1,0:T(4,128)} %get-tuple-element.5) | copy-start | bytes 196612
Sparse Core Ops, SparseCore 0:
  10.7 84.7 all-gather.2
